TPU v7x, 512 devices: a whole 4x8x8 slice. The times are simulated.
512 devices in a mesh: sp: 64 (over z, y), tp: 8 (over x, core).
Axes of the slice: x: 4, y: 8, z: 8, core: 2. Of those that a mesh axis runs over, the one named last changes fastest.
Arguments:
- tokens: bfloat16 [65536, 2048], P(('sp', 'tp')), may hold values from -6 to 6
- norm_gain: float32 [2048], replicated, may hold values from 0.1 to 1.9
- w_query: bfloat16 [2048, 2048], P('sp', 'tp'), may hold values from -0.125 to 0.125
- w_key: bfloat16 [2048, 2048], P('sp', 'tp'), may hold values from -0.125 to 0.125
- w_value: bfloat16 [2048, 4096], P('sp', 'tp'), may hold values from -0.125 to 0.125
- w_rank_down: bfloat16 [2048, 16], replicated, may hold values from -0.125 to 0.125
- w_rank_up: bfloat16 [16, 2048], P(None, 'tp'), may hold values from -1.5 to 1.5
- gate_bias: float32 [2048], P('tp')
- decay_shift: float32 [65536], P('sp'), may hold values from -1 to 0
- out_gain: float32 [512], replicated, may hold values from 0.1 to 1.9
- w_out: bfloat16 [4096, 2048], P('tp', 'sp'), may hold values from -0.09375 to 0.09375
Outputs:
- mixed: bfloat16 [65536, 2048], P(('sp', 'tp'))
All inputs are finite; a program needn't handle non-finite values.
Results may differ from a plain program's by a relative error of at most 0.015.
Values may be sent and summed in bfloat16 or wider, within the bound.
A program may use at most 128 MiB of HBM per device.

v0:
```python
import jax
import jax.numpy as jnp
from jax import lax
from jax.sharding import Mesh
from jax.sharding import PartitionSpec as P

DK = 256
DV = 512
TAU = 16
BLOCK = 64
SP = ("sp_0", "sp_1")
SP_TP = ("sp_0", "sp_1", "tp")
EPS = 1e-06


def sent_together(arrays, axis, dim, along):
    both = jnp.concatenate(arrays, axis=along)
    out, at, finished = (lax.all_gather(both, axis, axis=dim, tiled=True), 0, [])
    for a in arrays:
        finished.append(lax.slice_in_dim(out, at, at + a.shape[along], axis=along))
        at += a.shape[along]
    return tuple(finished)


def filled_with(value, identity):
    return jax.tree.map(
        lambda a, e: jnp.broadcast_to(jnp.asarray(e, a.dtype), a.shape), value, identity
    )


def entering(value, axes, combine, identity):
    before = start = filled_with(value, identity)
    total = value
    for axis in reversed(axes):
        size, mine = (lax.axis_size(axis), lax.axis_index(axis))
        pieces = jax.tree.map(lambda part: lax.all_gather(part, axis), total)
        inside, total = (start, start)
        for k in range(size):
            passed = k < mine
            total = combine(total, jax.tree.map(lambda part: part[k], pieces))
            inside = jax.tree.map(lambda new, old: jnp.where(passed, new, old), total, inside)
        before = combine(inside, before)
    return before


def cut_along(value, dim, size):
    before, after = (value.shape[:dim], value.shape[dim + 1 :])
    return jnp.moveaxis(value.reshape(*before, size, -1, *after), dim, 0)


def sent_and_summed(value, axis, dim):
    size = lax.axis_size(axis)
    parts = lax.all_to_all(cut_along(value, dim, size), axis, 0, 0, tiled=True)
    return jnp.sum(parts.astype(jnp.float32), axis=0)


def rms_rows(values, gain):
    wide = values.astype(jnp.float32)
    return wide * lax.rsqrt(jnp.mean(wide * wide, axis=-1, keepdims=True) + EPS) * gain


def local_pass(query, key, value, log_decay, state):
    rows, heads, width = query.shape
    blocks = rows // BLOCK

    def split(tensor):
        return tensor.reshape((blocks, BLOCK) + tensor.shape[1:])

    causal = jnp.tril(jnp.ones((BLOCK, BLOCK), dtype=bool))

    def local_step(carry, inputs):
        q_blk, k_blk, v_blk, g_blk = inputs
        cumul = jnp.cumsum(g_blk, axis=0)
        centre = cumul - cumul[BLOCK // 2]
        q_scaled = (q_blk * jnp.exp(centre)).astype(jnp.bfloat16)
        k_scaled = (k_blk * jnp.exp(-centre)).astype(jnp.bfloat16)
        scores = jnp.einsum("ihd,jhd->hij", q_scaled, k_scaled, preferred_element_type=jnp.float32)
        scores = jnp.where(causal[None], scores, 0.0).astype(jnp.bfloat16)
        within = jnp.einsum("hij,jhe->ihe", scores, v_blk, preferred_element_type=jnp.float32)
        final = cumul[-1]
        decayed = (k_blk * jnp.exp(final - cumul)).astype(jnp.bfloat16)
        nxt = jnp.exp(final)[:, :, None] * carry + jnp.einsum(
            "jhd,jhe->hde", decayed, v_blk, preferred_element_type=jnp.float32
        )
        return (nxt, (within, q_blk * jnp.exp(cumul), final, carry))

    carry, (within, reach, finals, starts) = lax.scan(
        local_step, state, (split(query), split(key), split(value), split(log_decay))
    )
    return (within, reach, finals, starts, carry)


def state_only(key, value, log_decay, state):
    rows, heads, width = key.shape
    blocks = rows // BLOCK

    def split(tensor):
        return tensor.reshape((blocks, BLOCK) + tensor.shape[1:])

    def state_step(carry, inputs):
        k_blk, v_blk, g_blk = inputs
        cumul = jnp.cumsum(g_blk, axis=0)
        final = cumul[-1]
        decayed = (k_blk * jnp.exp(final - cumul)).astype(jnp.bfloat16)
        carry = jnp.exp(final)[:, :, None] * carry + jnp.einsum(
            "jhd,jhe->hde", decayed, v_blk, preferred_element_type=jnp.float32
        )
        return (carry, final)

    carry, finals = lax.scan(state_step, state, (split(key), split(value), split(log_decay)))
    return (carry, finals)


def read_out(reach, starts):
    blocks, block, heads, width = reach.shape
    result = jnp.einsum(
        "nihd,nhde->nihe",
        reach.astype(jnp.bfloat16),
        starts.astype(jnp.bfloat16),
        preferred_element_type=jnp.float32,
    )
    return result.reshape(blocks * block, heads, -1)


def combine(earlier, later):
    return (earlier[0] * later[0], later[0][:, :, None] * earlier[1] + later[1])


def on_device(
    tokens,
    norm_gain,
    w_query,
    w_key,
    w_value,
    w_rank_down,
    w_rank_up,
    gate_bias,
    decay_shift,
    out_gain,
    w_out,
):
    normed = rms_rows(tokens, norm_gain).astype(jnp.bfloat16)
    query_w, key_w, value_w = sent_together((w_query, w_key, w_value), SP, 0, 1)
    keys_here = query_w.shape[1]
    vals_here = value_w.shape[1]
    heads_here = keys_here // DK
    w_joined = jnp.concatenate([query_w, key_w, value_w, w_rank_down], axis=1)
    joined = jnp.dot(
        lax.all_gather(normed, "tp", axis=0, tiled=True),
        w_joined,
        preferred_element_type=jnp.float32,
    ).astype(jnp.bfloat16)
    span = joined.shape[0]
    q_heads = joined[:, :keys_here].astype(jnp.float32).reshape(span, heads_here, DK) * DK ** (-0.5)
    k_heads = joined[:, keys_here : 2 * keys_here].astype(jnp.float32).reshape(span, heads_here, DK)
    v_heads = joined[:, 2 * keys_here : 2 * keys_here + vals_here].reshape(span, heads_here, DV)
    rank = joined[:, 2 * keys_here + vals_here :]
    pre = jnp.dot(rank, w_rank_up, preferred_element_type=jnp.float32) + gate_bias
    log_decay = (jax.nn.log_sigmoid(pre) / TAU + decay_shift[:, None]).reshape(span, heads_here, DK)
    empty = jnp.zeros((heads_here, DK, DV), jnp.float32)
    identity = (jnp.ones((heads_here, DK), jnp.float32), empty)
    local_end, finals = state_only(k_heads, v_heads, log_decay, empty)
    carried = entering((jnp.exp(jnp.sum(finals, axis=0)), local_end), SP, combine, identity)[1]
    within, reach, _, starts, _ = local_pass(q_heads, k_heads, v_heads, log_decay, carried)
    attended = within.reshape(span, heads_here, DV) + read_out(reach, starts)
    shaped = rms_rows(attended, out_gain).astype(jnp.bfloat16).reshape(span, heads_here * DV)
    out_whole = lax.all_gather(w_out, SP, axis=1, tiled=True)
    return sent_and_summed(
        jnp.dot(shaped, out_whole, preferred_element_type=jnp.float32).astype(jnp.bfloat16), "tp", 0
    ).astype(jnp.bfloat16)


def solution(mesh):
    finer = Mesh(mesh.devices.reshape(8, 8, mesh.shape["tp"]), ("sp_0", "sp_1", "tp"))
    in_specs = (
        P(SP_TP, None),
        P(),
        P(SP, "tp"),
        P(SP, "tp"),
        P(SP, "tp"),
        P(),
        P(None, "tp"),
        P("tp"),
        P(SP),
        P(),
        P("tp", SP),
    )
    out_specs = P(SP_TP, None)
    return jax.shard_map(
        on_device, mesh=finer, in_specs=in_specs, out_specs=out_specs, check_vma=False
    )
```

profile of v0, /device:TPU:1, one launch (start us, length us, event | category | flops | bytes accessed | tf_op | source)
XLA Modules:
  0.0 498.0 jit_solution(9612616746641343713)
XLA Ops:
  7.8 2.0 fusion.61
  12.5 40.7 %all-gather.9.cloned.1.call-done = bf16[1024,2048]{1,0:T(8,128)(2,1)} async-done(((bf16[128,2048]{1,0:T(8,128)(2,1)}), bf16[1024,2048]{1,0:T(8,128)(2,1)}) %all-gather.9.cloned.1.call-update) | async-done | bytes 4194320 | tf_op jit(solution)/shard_map/all_gather | solution.py:149
  53.2 85.4 %all-gather.11.cloned.1.call-done = bf16[2048,1024]{1,0:T(8,128)(2,1)} async-done(((bf16[32,1024]{1,0:T(8,128)(2,1)}), bf16[2048,1024]{1,0:T(8,128)(2,1)}) %all-gather.11.cloned.1.call-update) | async-done | bytes 4194320 | tf_op jit(solution)/shard_map/all_gather | solution.py:18
  138.6 8.1 %fusion.51 = bf16[1024,1040]{0,1:T(8,128)(2,1)S(1)} fusion(bf16[1024,2048]{1,0:T(8,128)(2,1)} %all-gather.9.cloned.1.call-done, bf16[2048,16]{1,0:T(8,128)(2,1)S(1)} %copy.37, bf16[2048,1024]{1,0:T(8,128)(2,1)} %all-gather.11.cloned.1.call-done), kind=kOutput, calls=%fused_computation.62 | convolution fusion | flops 4371660800 | bytes 10584064 | tf_op jit(solution)/shard_map/dot_general | solution.py:148
  148.0 1.9 fusion.64
  149.8 2.5 copy.39
  152.4 3.4 copy.42
  157.3 2.1 copy.43
  160.7 48.5 %while.31 = (s32[]{:T(128)}, f32[1,256,512]{2,1,0:T(8,128)S(1)}, f32[16,1,256]{2,1,0:T(1,128)S(1)}, f32[16,64,1,256]{3,2,1,0:T(1,128)}, f32[16,64,1,256]{3,2,1,0...) while((s32[]{:T(128)}, f32[1,256,512]{2,1,0:T(8,128)S(1)}, ...), condition=%wide.region_3.4_spmd.clone, body=%wide.region_1.3_spmd.clone.sunk | while | flops 18251780 | bytes 1450087 | solution.py:110
  210.2 11.0 %all-gather.2 = f32[8,1,256]{2,1,0:T(1,128)S(1)} all-gather(f32[1,1,256]{2,1,0:T(1,128)S(1)} %bitcast.299), channel_id=2, replica_groups=mesh['sp_0'=8,'sp_1'=8,'tp'=8] {'sp_1'}, dimensions={0}, use_global_device_ids=true | all-gather | bytes 9216 | tf_op jit(solution)/shard_map/all_gather | solution.py:36
  221.2 46.4 %all-gather.17.cloned.1.call-done = f32[8,256,512]{2,1,0:T(8,128)} async-done(((f32[1,256,512]{2,1,0:T(8,128)}), f32[8,256,512]{2,1,0:T(8,128)}) %all-gather.17.cloned.1.call-update) | async-done | bytes 4194320 | tf_op jit(solution)/shard_map/all_gather | solution.py:36
  267.6 3.3 bitcast_add_fusion.1
  271.7 13.7 %all_gather.30 = f32[8,1,256]{2,1,0:T(1,128)S(1)} all-gather(f32[1,1,256]{2,1,0:T(1,128)S(1)} %get-tuple-element.230), channel_id=1, replica_groups=mesh['sp_0'=8,'sp_1'=8,'tp'=8] {'sp_0'}, dimensions={0}, use_global_device_ids=true | all-gather | bytes 9216 | tf_op jit(solution)/shard_map/all_gather | solution.py:36
  285.7 42.6 %all-gather.13.cloned.1.call-done = f32[8,1,256,512]{3,2,1,0:T(8,128)} async-done(((f32[1,1,256,512]{3,2,1,0:T(8,128)}), f32[8,1,256,512]{3,2,1,0:T(8,128)}) %all-gather.13.cloned.1.call-update) | async-done | bytes 4194320 | tf_op jit(solution)/shard_map/all_gather | solution.py:36
  328.3 4.3 fusion.68
  332.6 93.2 %while.30 = (s32[]{:T(128)}, f32[1,256,512]{2,1,0:T(8,128)S(1)}, f32[16,64,1,512]{3,1,2,0:T(8,128)}, bf16[16,64,1,256]{3,1,0,2:T(8,128)(2,1)S(1)}, bf16[16,1,256...) while((s32[]{:T(128)}, f32[1,256,512]{2,1,0:T(8,128)S(1)}, ...), condition=%wide.region_7.8_spmd.clone, body=%wide.region_5.7_spmd.clone.sunk | while | flops 24555520 | bytes 3223153 | solution.py:87
  340.6 1.8 fusion.117
  346.4 1.8 fusion.117
  363.9 1.8 fusion.117
  404.7 1.8 fusion.117
  425.8 3.8 multiply_reduce_fusion
  430.0 4.0 convolution_convert_fusion
  434.0 53.6 %all_to_all.5 = bf16[8,128,2048]{2,1,0:T(8,128)(2,1)} all-to-all(bf16[8,128,2048]{2,1,0:T(8,128)(2,1)S(1)} %bitcast.263), channel_id=1, replica_groups=mesh['sp_0'=8,'sp_1'=8,'tp'=8] {'tp'}, dimensions={0} | all-to-all | bytes 8388608 | tf_op jit(solution)/shard_map/all_to_all | solution.py:53
  487.7 3.8 reduce_sum.42
  (273 shorter events, 143.4 us)
Async XLA Ops:
  6.5 141.4 %copy-start = (bf16[16,256]{1,0:T(8,128)(2,1)S(1)}, bf16[16,256]{1,0:T(8,128)(2,1)}, u32[]{:S(2)}) copy-start(bf16[16,256]{1,0:T(8,128)(2,1)} %param.21) | copy-start | bytes 24580
  6.5 46.7 %all-gather.9.cloned.1.call-start = ((), (), s32[]{:S(2)}) async-start(), calls=%async_computation.1 | async-start | bytes 4718592 | tf_op jit(solution)/shard_map/all_gather | solution.py:149
  9.8 128.8 %all-gather.11.cloned.1.call-start = ((), (), s32[]{:S(2)}) async-start(), calls=%async_computation.2 | async-start | bytes 4259840 | tf_op jit(solution)/shard_map/all_gather | solution.py:18
  11.3 256.3 %all-gather.17.cloned.1.call-start = ((), (), s32[]{:S(2)}) async-start(), calls=%async_computation.5 | async-start | bytes 4718592 | tf_op jit(solution)/shard_map/all_gather | solution.py:36
  12.5 135.5 %copy-start.6 = (f32[1024]{0:T(1024)S(1)}, f32[1024]{0:T(1024)}, u32[]{:S(2)}) copy-start(f32[1024]{0:T(1024)} %param.23) | copy-start | bytes 12292
  12.5 135.4 %copy-start.7 = (f32[256]{0:T(256)S(1)}, f32[256]{0:T(256)}, u32[]{:S(2)}) copy-start(f32[256]{0:T(256)} %param.22) | copy-start | bytes 3076
  146.7 5.6 %copy-start.2 = (bf16[1024,1040]{0,1:T(8,128)(2,1)}, bf16[1024,1040]{0,1:T(8,128)(2,1)S(1)}, u32[]{:S(2)}) copy-start(bf16[1024,1040]{0,1:T(8,128)(2,1)S(1)} %fusion.51) | copy-start | bytes 6389764
  152.4 7.1 %slice-start = ((bf16[1024,1040]{0,1:T(8,128)(2,1)}), bf16[1024,512]{0,1:T(8,128)(2,1)S(1)}, s32[]{:S(2)}) async-start(bf16[1024,1040]{0,1:T(8,128)(2,1)} %copy-done.2), calls=%async_computation.6 | async-start | bytes 2097152 | tf_op jit(solution)/shard_map/slice | solution.py:156
  209.2 0.8 copy-start.1
  209.2 62.3 %copy-start.3 = (bf16[1024,1040]{0,1:T(8,128)(2,1)S(1)}, bf16[1024,1040]{0,1:T(8,128)(2,1)}, u32[]{:S(2)}) copy-start(bf16[1024,1040]{0,1:T(8,128)(2,1)} %copy-done.2) | copy-start | bytes 6389764
  210.0 118.2 %all-gather.13.cloned.1.call-start = ((), (), s32[]{:S(2)}) async-start(), calls=%async_computation.3 | async-start | bytes 4718592 | tf_op jit(solution)/shard_map/all_gather | solution.py:36
  270.9 159.1 %all-gather.15.cloned.1.call-start = ((), (), s32[]{:S(2)}) async-start(), calls=%async_computation.4 | async-start | bytes 2129920 | tf_op jit(solution)/shard_map/all_gather | solution.py:167
  328.3 4.3 copy-start.4
  425.8 3.9 copy-start.5
Sparse Core Ops, SparseCore 0:
  10.0 43.2 all-gather.8
  56.3 82.2 all-gather.10
  210.2 57.3 all-gather.16
  271.0 57.2 all-gather.12
  331.2 77.5 all-gather.14
where the time goes:
time: 504 us; the launch traced here: 498 us
  waiting for transfers between devices  216 us (43%)
  matrix products  82.2 us (16%)
  other arithmetic  81 us (16%)
  blocking collectives  78.3 us (16%)
  local copies, waits for them, and re-layouts  25.8 us (5%)
  between operations  13.4 us (3%)
    all_gather x2, waiting for transfers between devices, entering(): pieces = jax.tree.map(lambda part: lax.all_gather(part, axis), total)  89 us
    all_gather x1, waiting for transfers between devices, sent_together(): lax.all_gather(both, axis, axis=dim, tiled=True)  85.4 us
    all_to_all x1, blocking collectives, sent_and_summed(): parts = lax.all_to_all(cut_along(value, dim, size), axis, 0, 0, tiled=True)  53.6 us
    all_gather x1, waiting for transfers between devices, on_device(): lax.all_gather(normed, 'tp', axis=0, tiled=True)  40.7 us
    dot_general x16, matrix products, local_step(): jnp.einsum('hij,jhe->ihe', scores, v_blk, preferred_element_type=jnp.floa...  28.5 us
    all_gather x2, blocking collectives, entering(): pieces = jax.tree.map(lambda part: lax.all_gather(part, axis), total)  24.7 us
    dot_general x16, matrix products, local_step(): jnp.einsum('jhd,jhe->hde', decayed, v_blk, preferred_element_type=jnp.flo...  18.3 us
    dot_general x16, matrix products, state_step(): jnp.einsum('jhd,jhe->hde', decayed, v_blk, preferred_element_type=jnp.flo...  17.7 us
  transfers between devices with their start and end apart: 5, of which 4 were waited for; matrix products, arithmetic and copies ran while one was open for 21% of the time, Pallas kernels for 0%

commit v1 on v0

--- a/solution.py
+++ b/solution.py
@@ -11,6 +11,14 @@
 SP = ("sp_0", "sp_1")
 SP_TP = ("sp_0", "sp_1", "tp")
 EPS = 1e-06
+
+
+def tiled_gather(shard, axis, dim):
+    size = lax.axis_size(axis)
+    repeats = [size if d == dim else 1 for d in range(shard.ndim)]
+    return lax.all_to_all(
+        jnp.tile(shard, repeats), axis, split_axis=dim, concat_axis=dim, tiled=True
+    )
 
 
 def sent_together(arrays, axis, dim, along):
@@ -146,9 +154,7 @@
     heads_here = keys_here // DK
     w_joined = jnp.concatenate([query_w, key_w, value_w, w_rank_down], axis=1)
     joined = jnp.dot(
-        lax.all_gather(normed, "tp", axis=0, tiled=True),
-        w_joined,
-        preferred_element_type=jnp.float32,
+        tiled_gather(normed, "tp", 0), w_joined, preferred_element_type=jnp.float32
     ).astype(jnp.bfloat16)
     span = joined.shape[0]
     q_heads = joined[:, :keys_here].astype(jnp.float32).reshape(span, heads_here, DK) * DK ** (-0.5)

time: 504 us -> 464 us (0.921)
  waiting for transfers between devices: 216 us -> 164 us
  starting transfers between devices: 0.17 us -> 11.5 us
    all_gather x1, waiting for transfers between devices: 85.4 us -> 25.4 us  [sent_together(): lax.all_gather(both, axis, axis=dim, tiled=True)]
    all_to_all x0 -> x1, waiting for transfers between devices: none -> 48.5 us  [tiled_gather(): lax.all_to_all(jnp.tile(shard, repeats), axis, split_axis=dim, concat_axi...]
    all_gather x1 -> x0, waiting for transfers between devices: 40.7 us -> none  [on_device(): lax.all_gather(normed, 'tp', axis=0, tiled=True)]
    all_to_all x0 -> x1, starting transfers between devices: none -> 11.4 us  [tiled_gather(): lax.all_to_all(jnp.tile(shard, repeats), axis, split_axis=dim, concat_axi...]
  transfers between devices with their start and end apart: 5 -> 5, of which waited for: 4 -> 4; matrix products, arithmetic and copies ran while one was open for 21% -> 23% of each run, Pallas kernels for 0% -> 0%
where the time goes in v1:
time: 464 us; the launch traced here: 458 us
  waiting for transfers between devices  164 us (35%)
  matrix products  82.2 us (18%)
  other arithmetic  80.2 us (17%)
  blocking collectives  78.3 us (17%)
  local copies, waits for them, and re-layouts  27.5 us (6%)
  between operations  13.4 us (3%)
  starting transfers between devices  11.5 us (2%)
    all_gather x2, waiting for transfers between devices, entering(): pieces = jax.tree.map(lambda part: lax.all_gather(part, axis), total)  89 us
    all_to_all x1, blocking collectives, sent_and_summed(): parts = lax.all_to_all(cut_along(value, dim, size), axis, 0, 0, tiled=True)  53.6 us
    all_to_all x1, waiting for transfers between devices, tiled_gather(): lax.all_to_all(jnp.tile(shard, repeats), axis, split_axis=dim, concat_axi...  48.5 us
    dot_general x16, matrix products, local_step(): jnp.einsum('hij,jhe->ihe', scores, v_blk, preferred_element_type=jnp.floa...  28.5 us
    all_gather x1, waiting for transfers between devices, sent_together(): lax.all_gather(both, axis, axis=dim, tiled=True)  25.4 us
    all_gather x2, blocking collectives, entering(): pieces = jax.tree.map(lambda part: lax.all_gather(part, axis), total)  24.7 us
    dot_general x16, matrix products, local_step(): jnp.einsum('jhd,jhe->hde', decayed, v_blk, preferred_element_type=jnp.flo...  18.3 us
    dot_general x16, matrix products, state_step(): jnp.einsum('jhd,jhe->hde', decayed, v_blk, preferred_element_type=jnp.flo...  17.7 us
  transfers between devices with their start and end apart: 5, of which 4 were waited for; matrix products, arithmetic and copies ran while one was open for 23% of the time, Pallas kernels for 0%

profile of v1, /device:TPU:1, one launch (start us, length us, event | category | flops | bytes accessed | tf_op | source)
XLA Modules:
  0.0 458.0 jit_solution(4430962109284820241)
XLA Ops:
  10.4 2.5 tile.2
  12.9 11.4 %all-to-all-start = ((bf16[8,128,2048]{2,1,0:T(8,128)(2,1)}), bf16[8,128,2048]{2,1,0:T(8,128)(2,1)}, u32[]{:S(2)}, u32[]{:S(2)}) async-start(bf16[8,128,2048]{2,1,0:T(8,128)(2,1)} %tile.2), calls=%async_computation | async-start | bytes 8388608 | tf_op jit(solution)/shard_map/all_to_all | solution.py:19
  24.6 48.5 %all-to-all-done = bf16[8,128,2048]{2,1,0:T(8,128)(2,1)} async-done(((bf16[8,128,2048]{2,1,0:T(8,128)(2,1)}), bf16[8,128,2048]{2,1,0:T(8,128)(2,1)}, u32[]{:S(2)}, u32[]{:S(2)}) %all-to-all-start) | async-done | bytes 4194336 | tf_op jit(solution)/shard_map/all_to_all | solution.py:19
  73.2 25.4 %all-gather.8.cloned.1.call-done = bf16[2048,1024]{1,0:T(8,128)(2,1)} async-done(((bf16[32,1024]{1,0:T(8,128)(2,1)}), bf16[2048,1024]{1,0:T(8,128)(2,1)}) %all-gather.8.cloned.1.call-update) | async-done | bytes 4194320 | tf_op jit(solution)/shard_map/all_gather | solution.py:26
  98.6 8.1 %fusion.51 = bf16[1024,1040]{0,1:T(8,128)(2,1)S(1)} fusion(bf16[1024,2048]{1,0:T(8,128)(2,1)} %bitcast, bf16[2048,16]{1,0:T(8,128)(2,1)S(1)} %copy.37, bf16[2048,1024]{1,0:T(8,128)(2,1)} %all-gather.8.cloned.1.call-done), kind=kOutput, calls=%fused_computation.62 | convolution fusion | flops 4371660800 | bytes 10584064 | tf_op jit(solution)/shard_map/dot_general | solution.py:156
  107.9 1.9 fusion.64
  109.8 2.5 copy.39
  112.3 3.4 copy.42
  117.3 2.1 copy.43
  120.7 48.5 %while.31 = (s32[]{:T(128)}, f32[1,256,512]{2,1,0:T(8,128)S(1)}, f32[16,1,256]{2,1,0:T(1,128)S(1)}, f32[16,64,1,256]{3,2,1,0:T(1,128)}, f32[16,64,1,256]{3,2,1,0...) while((s32[]{:T(128)}, f32[1,256,512]{2,1,0:T(8,128)S(1)}, ...), condition=%wide.region_3.4_spmd.clone, body=%wide.region_1.3_spmd.clone.sunk | while | flops 18251780 | bytes 1450087 | solution.py:118
  170.1 11.0 %all-gather.2 = f32[8,1,256]{2,1,0:T(1,128)S(1)} all-gather(f32[1,1,256]{2,1,0:T(1,128)S(1)} %bitcast.300), channel_id=2, replica_groups=mesh['sp_0'=8,'sp_1'=8,'tp'=8] {'sp_1'}, dimensions={0}, use_global_device_ids=true | all-gather | bytes 9216 | tf_op jit(solution)/shard_map/all_gather | solution.py:44
  181.2 46.4 %all-gather.14.cloned.1.call-done = f32[8,256,512]{2,1,0:T(8,128)} async-done(((f32[1,256,512]{2,1,0:T(8,128)}), f32[8,256,512]{2,1,0:T(8,128)}) %all-gather.14.cloned.1.call-update) | async-done | bytes 4194320 | tf_op jit(solution)/shard_map/all_gather | solution.py:44
  227.6 3.3 bitcast_add_fusion.1
  231.6 13.7 %all_gather.26 = f32[8,1,256]{2,1,0:T(1,128)S(1)} all-gather(f32[1,1,256]{2,1,0:T(1,128)S(1)} %get-tuple-element.230), channel_id=1, replica_groups=mesh['sp_0'=8,'sp_1'=8,'tp'=8] {'sp_0'}, dimensions={0}, use_global_device_ids=true | all-gather | bytes 9216 | tf_op jit(solution)/shard_map/all_gather | solution.py:44
  245.7 42.6 %all-gather.10.cloned.1.call-done = f32[8,1,256,512]{3,2,1,0:T(8,128)} async-done(((f32[1,1,256,512]{3,2,1,0:T(8,128)}), f32[8,1,256,512]{3,2,1,0:T(8,128)}) %all-gather.10.cloned.1.call-update) | async-done | bytes 4194320 | tf_op jit(solution)/shard_map/all_gather | solution.py:44
  288.3 4.3 fusion.68
  292.6 93.2 %while.30 = (s32[]{:T(128)}, f32[1,256,512]{2,1,0:T(8,128)S(1)}, f32[16,64,1,512]{3,1,2,0:T(8,128)}, bf16[16,64,1,256]{3,1,0,2:T(8,128)(2,1)S(1)}, bf16[16,1,256...) while((s32[]{:T(128)}, f32[1,256,512]{2,1,0:T(8,128)S(1)}, ...), condition=%wide.region_7.8_spmd.clone, body=%wide.region_5.7_spmd.clone.sunk | while | flops 24555520 | bytes 3223153 | solution.py:95
  306.4 1.8 fusion.117
  323.9 1.8 fusion.117
  364.6 1.8 fusion.117
  385.8 3.8 multiply_reduce_fusion
  390.0 4.0 convolution_convert_fusion
  394.0 53.6 %all_to_all.14 = bf16[8,128,2048]{2,1,0:T(8,128)(2,1)} all-to-all(bf16[8,128,2048]{2,1,0:T(8,128)(2,1)S(1)} %bitcast.264), channel_id=1, replica_groups=mesh['sp_0'=8,'sp_1'=8,'tp'=8] {'tp'}, dimensions={0} | all-to-all | bytes 8388608 | tf_op jit(solution)/shard_map/all_to_all | solution.py:61
  447.6 3.8 reduce_sum.42
  (275 shorter events, 145.5 us)
Async XLA Ops:
  6.5 101.4 %copy-start = (bf16[16,256]{1,0:T(8,128)(2,1)S(1)}, bf16[16,256]{1,0:T(8,128)(2,1)}, u32[]{:S(2)}) copy-start(bf16[16,256]{1,0:T(8,128)(2,1)} %param.21) | copy-start | bytes 24580
  6.5 92.0 %all-gather.8.cloned.1.call-start = ((), (), s32[]{:S(2)}) async-start(), calls=%async_computation.2 | async-start | bytes 4259840 | tf_op jit(solution)/shard_map/all_gather | solution.py:26
  12.9 11.4 %copy-start.5 = (bf16[2048,16]{0,1:T(8,128)(2,1)S(1)}, bf16[2048,16]{0,1:T(8,128)(2,1)}, u32[]{:S(2)}) copy-start(bf16[2048,16]{0,1:T(8,128)(2,1)} %param.20) | copy-start | bytes 196612
  12.9 60.2 %all-to-all-start = ((bf16[8,128,2048]{2,1,0:T(8,128)(2,1)}), bf16[8,128,2048]{2,1,0:T(8,128)(2,1)}, u32[]{:S(2)}, u32[]{:S(2)}) async-start(bf16[8,128,2048]{2,1,0:T(8,128)(2,1)} %tile.2), calls=%async_computation | async-start | bytes 8388608 | tf_op jit(solution)/shard_map/all_to_all | solution.py:19
  24.3 203.2 %all-gather.14.cloned.1.call-start = ((), (), s32[]{:S(2)}) async-start(), calls=%async_computation.5 | async-start | bytes 4718592 | tf_op jit(solution)/shard_map/all_gather | solution.py:44
  98.6 9.4 %copy-start.7 = (f32[1024]{0:T(1024)S(1)}, f32[1024]{0:T(1024)}, u32[]{:S(2)}) copy-start(f32[1024]{0:T(1024)} %param.23) | copy-start | bytes 12292
  98.6 9.4 %copy-start.8 = (f32[256]{0:T(256)S(1)}, f32[256]{0:T(256)}, u32[]{:S(2)}) copy-start(f32[256]{0:T(256)} %param.22) | copy-start | bytes 3076
  106.7 5.6 %copy-start.2 = (bf16[1024,1040]{0,1:T(8,128)(2,1)}, bf16[1024,1040]{0,1:T(8,128)(2,1)S(1)}, u32[]{:S(2)}) copy-start(bf16[1024,1040]{0,1:T(8,128)(2,1)S(1)} %fusion.51) | copy-start | bytes 6389764
  112.3 7.1 %slice-start = ((bf16[1024,1040]{0,1:T(8,128)(2,1)}), bf16[1024,512]{0,1:T(8,128)(2,1)S(1)}, s32[]{:S(2)}) async-start(bf16[1024,1040]{0,1:T(8,128)(2,1)} %copy-done.2), calls=%async_computation.6 | async-start | bytes 2097152 | tf_op jit(solution)/shard_map/slice | solution.py:162
  169.2 0.8 copy-start.1
  169.2 62.3 %copy-start.3 = (bf16[1024,1040]{0,1:T(8,128)(2,1)S(1)}, bf16[1024,1040]{0,1:T(8,128)(2,1)}, u32[]{:S(2)}) copy-start(bf16[1024,1040]{0,1:T(8,128)(2,1)} %copy-done.2) | copy-start | bytes 6389764
  170.0 118.2 %all-gather.10.cloned.1.call-start = ((), (), s32[]{:S(2)}) async-start(), calls=%async_computation.3 | async-start | bytes 4718592 | tf_op jit(solution)/shard_map/all_gather | solution.py:44
  230.9 159.1 %all-gather.12.cloned.1.call-start = ((), (), s32[]{:S(2)}) async-start(), calls=%async_computation.4 | async-start | bytes 2129920 | tf_op jit(solution)/shard_map/all_gather | solution.py:173
  288.3 4.3 copy-start.4
  385.8 3.9 copy-start.6
Sparse Core Ops, SparseCore 0:
  10.4 88.1 all-gather.7
  170.1 57.3 all-gather.13
  231.0 57.2 all-gather.9
  291.2 77.5 all-gather.11
